TPU v7x, 32 devices: a whole 2x2x4 slice. The times are simulated.
32 devices in a mesh: kv: 8 (over z, y), tp: 4 (over x, core).
Axes of the slice: x: 2, y: 2, z: 4, core: 2. Of those that a mesh axis runs over, the one named last changes fastest.
Arguments:
- tokens: bfloat16 [256, 4, 2048], P(None, None, ('kv', 'tp')), may hold values from -520 to 520
- input_norm_gain: bfloat16 [2048], replicated, may hold values from 0.099609375 to 1.8984375
- query_weight: bfloat16 [2048, 2048], P(None, 'kv'), may hold values from -0.125 to 0.125
- key_weight: bfloat16 [2048, 2048], P(None, 'kv'), may hold values from -0.125 to 0.125
- value_weight: bfloat16 [2048, 16, 128], P(None, 'kv', 'tp'), may hold values from -1.14904852 to 1.14904852
- output_gate_weight: bfloat16 [2048, 16, 128], P(None, 'kv', 'tp'), may hold values from -0.125 to 0.125
- strength_weight: bfloat16 [2048, 16], P(None, 'kv'), may hold values from -0.125 to 0.125
- decay_weight: bfloat16 [2048, 16], P(None, 'kv'), may hold values from -0.125 to 0.125
- head_decay_rate: float32 [16], P('kv'), may hold values from 0.005 to 1.5
- proposal_log_decay: float32 [256, 4, 16], P(None, None, 'kv'), may hold values from -0.69 to 0
- head_norm_gain: bfloat16 [128], P('tp'), may hold values from 0.099609375 to 1.8984375
- output_weight: bfloat16 [16, 128, 2048], P('kv', 'tp'), may hold values from -1.14904852 to 1.14904852
- output_norm_gain: bfloat16 [2048], P(('kv', 'tp')), may hold values from 0.099609375 to 1.8984375
- state: float32 [256, 16, 128, 128], P(None, 'kv', 'tp'), may hold values from -4.5961941 to 4.5961941
- previous_keys: bfloat16 [256, 4, 2048], P(None, None, 'kv'), may hold values from -6 to 6
- previous_values: bfloat16 [256, 4, 16, 128], P(None, None, 'kv', 'tp'), may hold values from -52 to 52
- previous_log_decay: float32 [256, 4, 16], P(None, None, 'kv'), may hold values from -0.7 to -0.02
- previous_strengths: float32 [256, 4, 16], P(None, None, 'kv'), may hold values from 0.1 to 0.9
- accepted: int32 [256], replicated, may hold values from 0 to 4
- parent: int32 [256, 4], replicated, may hold values from -1 to 2, as said below
Outputs:
- layer_out: bfloat16 [256, 4, 2048], P(None, None, ('kv', 'tp'))
- accepted_state: float32 [256, 16, 128, 128], P(None, 'kv', 'tp')
Inputs may be any that keep to these rules, and one draw needn't show every extreme that they name: parent[b, i] is -1 or a proposal index below i; -1 means that proposal i follows the accepted old proposals directly.
All inputs are finite; a program needn't handle non-finite values.
Results may differ from a plain program's by a relative error of at most 0.019.
Values may be sent and summed in bfloat16 or wider, within the bound.
A program may use at most 128 MiB of HBM per device.

v0:
```python
import jax
import jax.numpy as jnp
from jax import lax
from jax.sharding import PartitionSpec as P

epsilon = 1e-06


def unit_rows(matrix):
    return matrix * lax.rsqrt(jnp.sum(matrix * matrix, axis=-1, keepdims=True) + epsilon)


def exact_product(form, left, right):
    return jnp.einsum(form, left, right, precision=lax.Precision.HIGHEST)


def visibility(parent):
    sequence_count, proposal_count = parent.shape
    position = jnp.arange(proposal_count, dtype=jnp.int32)
    parent_hot = (parent[:, :, None] == position[None, None, :]).astype(jnp.float32)
    ancestry = []
    for row_index in range(proposal_count):
        ancestor_row = parent_hot[:, row_index, :]
        if row_index > 0:
            earlier = jnp.stack(ancestry, axis=1)
            ancestor_row = ancestor_row + exact_product(
                "bj,bjk->bk", parent_hot[:, row_index, :row_index], earlier
            )
        ancestry.append(ancestor_row)
    ancestor = jnp.stack(ancestry, axis=1)
    chain = (position[:, None] > position[None, :]).astype(jnp.float32)
    upper = jnp.concatenate(
        [
            jnp.broadcast_to(chain, (sequence_count, proposal_count, proposal_count)),
            jnp.zeros((sequence_count, proposal_count, proposal_count), jnp.float32),
        ],
        axis=2,
    )
    lower = jnp.concatenate(
        [jnp.ones((sequence_count, proposal_count, proposal_count), jnp.float32), ancestor], axis=2
    )
    return jnp.concatenate([upper, lower], axis=1)


def split_heads(matrix, sequence_count, proposal_count, number_of_heads):
    return (
        matrix.astype(jnp.float32)
        .reshape(sequence_count, proposal_count, number_of_heads, -1)
        .transpose(0, 2, 1, 3)
    )


def delta_recursion(
    query_projected,
    key_projected,
    value_projected,
    output_gate_logits,
    write_strength_logits,
    decay_logits,
    decay_speed,
    proposal_group,
    head_norm_gain,
    state,
    previous_keys,
    previous_values,
    previous_log_decay,
    previous_strengths,
    accepted,
    parent,
    channel_count_total,
):
    sequence_count, number_of_heads, value_dim, head_dim = state.shape
    proposal_count = parent.shape[1]
    queries = unit_rows(
        split_heads(query_projected, sequence_count, proposal_count, number_of_heads)
    ) * head_dim ** (-0.5)
    new_keys = unit_rows(
        split_heads(key_projected, sequence_count, proposal_count, number_of_heads)
    )
    old_keys = unit_rows(
        split_heads(previous_keys, sequence_count, proposal_count, number_of_heads)
    )
    new_values = split_heads(value_projected, sequence_count, proposal_count, number_of_heads)
    old_values = split_heads(previous_values, sequence_count, proposal_count, number_of_heads)
    zgate = split_heads(output_gate_logits, sequence_count, proposal_count, number_of_heads)
    beta_new = jax.nn.sigmoid(
        write_strength_logits.reshape(sequence_count, proposal_count, number_of_heads)
    ).transpose(0, 2, 1)
    fresh_decay = (
        -decay_speed[None, None, :]
        * jax.nn.softplus(decay_logits.reshape(sequence_count, proposal_count, number_of_heads))
        + proposal_group
    ).transpose(0, 2, 1)
    position = jnp.arange(proposal_count, dtype=jnp.int32)
    live = (position[None, :] < accepted[:, None]).astype(jnp.float32)[:, None, :]
    beta_old = previous_strengths.transpose(0, 2, 1) * live
    decay_old = previous_log_decay.transpose(0, 2, 1) * live
    keys_all = jnp.concatenate([old_keys, new_keys], axis=2)
    values_all = jnp.concatenate([old_values, new_values], axis=2)
    beta_all = jnp.concatenate([beta_old, beta_new], axis=2)
    decay_all = jnp.concatenate([decay_old, fresh_decay], axis=2)
    visible = visibility(parent)
    gamma_sum = decay_all + exact_product("bij,bhj->bhi", visible, decay_all)
    gamma_diff = gamma_sum[:, :, :, None] - gamma_sum[:, :, None, :]
    decay_pair = jnp.exp(jnp.minimum(gamma_diff, 0.0)) * visible[:, None]
    coupling = (
        beta_all[..., None] * exact_product("bhid,bhjd->bhij", keys_all, keys_all) * decay_pair
    )
    right_side = jnp.concatenate(
        [beta_all[..., None] * values_all, (beta_all * jnp.exp(gamma_sum))[..., None] * keys_all],
        axis=-1,
    )
    solved = []
    for row_index in range(2 * proposal_count):
        current = right_side[:, :, row_index]
        if row_index > 0:
            current = current - exact_product(
                "bhj,bhjd->bhd", coupling[:, :, row_index, :row_index], jnp.stack(solved, axis=2)
            )
        solved.append(current)
    solution = jnp.stack(solved, axis=2)
    update = solution[..., :value_dim] - exact_product(
        "bhcd,bhed->bhce", solution[..., value_dim:], state
    )
    identity = jnp.eye(2 * proposal_count, dtype=jnp.float32)
    seen = visible[:, proposal_count:] + identity[proposal_count:][None]
    reach = jnp.exp(jnp.minimum(gamma_diff[:, :, proposal_count:], 0.0)) * seen[:, None]
    query_key = exact_product("bhid,bhjd->bhij", queries, keys_all) * reach
    readout = exact_product(
        "bhid,bhed->bhie", queries * jnp.exp(gamma_sum[:, :, proposal_count:])[..., None], state
    )
    readout = readout + exact_product("bhij,bhje->bhie", query_key, update)
    squares = channel_count_total(jnp.sum(readout * readout, axis=-1))
    readout = readout * lax.rsqrt(squares / head_dim + epsilon)[..., None]
    readout = readout * head_norm_gain.astype(jnp.float32) * jax.nn.silu(zgate)
    blended_rows = readout.transpose(0, 2, 1, 3).reshape(
        sequence_count * proposal_count, number_of_heads * value_dim
    )
    blended_rows = blended_rows.astype(jnp.bfloat16)
    last_gamma = gamma_sum[:, :, proposal_count - 1 : proposal_count]
    key_weighted = old_keys * jnp.exp(last_gamma - gamma_sum[:, :, :proposal_count])[..., None]
    accepted_state = jnp.exp(last_gamma)[..., None] * state + exact_product(
        "bhcd,bhce->bhed", key_weighted, update[:, :, :proposal_count]
    )
    return (blended_rows, accepted_state)


def channel_sum(squares):
    return lax.psum(squares, "tp")


def on_device(
    tokens,
    input_norm_gain,
    query_weight,
    key_weight,
    value_weight,
    output_gate_weight,
    strength_weight,
    decay_weight,
    head_decay_rate,
    proposal_log_decay,
    head_norm_gain,
    output_weight,
    output_norm_gain,
    state,
    previous_keys,
    previous_values,
    previous_log_decay,
    previous_strengths,
    accepted,
    parent,
):
    gathered = lax.all_gather(tokens, ("kv", "tp"), axis=2, tiled=True)
    sequence_count, proposal_count, width = gathered.shape
    row_total = sequence_count * proposal_count
    features = gathered.astype(jnp.float32)
    normed = features * lax.rsqrt(jnp.mean(features * features, axis=-1, keepdims=True) + epsilon)
    normed = (normed * input_norm_gain.astype(jnp.float32)).astype(jnp.bfloat16)
    flat_rows = normed.reshape(row_total, width)
    write_strength_logits = jnp.dot(flat_rows, strength_weight, preferred_element_type=jnp.float32)
    decay_logits = jnp.dot(flat_rows, decay_weight, preferred_element_type=jnp.float32)
    value_projected = jnp.dot(
        flat_rows, value_weight.reshape(width, -1), preferred_element_type=jnp.float32
    ).astype(jnp.bfloat16)
    output_gate_logits = jnp.dot(
        flat_rows, output_gate_weight.reshape(width, -1), preferred_element_type=jnp.float32
    ).astype(jnp.bfloat16)
    query_projected = jnp.dot(flat_rows, query_weight, preferred_element_type=jnp.float32).astype(
        jnp.bfloat16
    )
    key_projected = jnp.dot(flat_rows, key_weight, preferred_element_type=jnp.float32).astype(
        jnp.bfloat16
    )
    blended_rows, accepted_state = delta_recursion(
        query_projected,
        key_projected,
        value_projected,
        output_gate_logits,
        write_strength_logits,
        decay_logits,
        head_decay_rate,
        proposal_log_decay,
        head_norm_gain,
        state,
        previous_keys,
        previous_values,
        previous_log_decay,
        previous_strengths,
        accepted,
        parent,
        channel_sum,
    )
    partial_out = jnp.dot(
        blended_rows, output_weight.reshape(-1, width), preferred_element_type=jnp.float32
    )
    own_cols = output_norm_gain.shape[0]
    totals = lax.psum(partial_out, ("kv", "tp"))
    scaling = lax.rsqrt(jnp.mean(totals * totals, axis=-1, keepdims=True) + epsilon)
    own_index = lax.axis_index("kv") * lax.axis_size("tp") + lax.axis_index("tp")
    share = lax.dynamic_slice_in_dim(totals, own_index * own_cols, own_cols, 1)
    layer_out = (share * scaling * output_norm_gain.astype(jnp.float32)).astype(jnp.bfloat16)
    return (layer_out.reshape(sequence_count, proposal_count, own_cols), accepted_state)


def solution(mesh):
    placed = (
        P(None, None, ("kv", "tp")),
        P(),
        P(None, "kv"),
        P(None, "kv"),
        P(None, "kv", "tp"),
        P(None, "kv", "tp"),
        P(None, "kv"),
        P(None, "kv"),
        P("kv"),
        P(None, None, "kv"),
        P("tp"),
        P("kv", "tp", None),
        P(("kv", "tp")),
        P(None, "kv", "tp", None),
        P(None, None, "kv"),
        P(None, None, "kv", "tp"),
        P(None, None, "kv"),
        P(None, None, "kv"),
        P(),
        P(),
    )
    return jax.shard_map(
        on_device,
        mesh=mesh,
        in_specs=placed,
        out_specs=(P(None, None, ("kv", "tp")), P(None, "kv", "tp", None)),
        check_vma=False,
    )
```

profile of v0, /device:TPU:0, one launch (start us, length us, event | category | flops | bytes accessed | tf_op | source)
XLA Modules:
  0.0 489.5 jit_solution(4462959712660813374)
XLA Ops:
  17.7 58.3 %all-gather.2.cloned.1.call-done = bf16[256,4,2048]{0,2,1:T(8,128)(2,1)} async-done(((bf16[256,4,64]{0,2,1:T(8,128)(2,1)}), bf16[256,4,2048]{0,2,1:T(8,128)(2,1)}) %all-gather.2.cloned.1.call-update) | async-done | bytes 4194320 | tf_op jit(solution)/shard_map/all_gather | solution.py:174
  76.1 3.2 fusion
  79.5 2.7 fusion.2
  82.2 7.9 %copy.594 = bf16[256,4,2048]{2,1,0:T(4,128)(2,1)} copy(bf16[256,4,2048]{0,2,1:T(8,128)(2,1)} %fusion.2) | data formatting | bytes 8388608 | tf_op jit(solution)/shard_map/convert_element_type | solution.py:179
  90.2 3.0 fusion.61
  98.4 6.9 %reshape.134 = bf16[1024,2048]{1,0:T(8,128)(2,1)} reshape(bf16[256,4,2048]{2,1,0:T(4,128)(2,1)} %copy.594) | data formatting | bytes 8388608 | tf_op jit(solution)/shard_map/reshape | solution.py:180
  105.2 3.4 fusion.9
  115.3 5.3 %multiply_multiply_fusion = f32[256,2,8,8]{3,2,1,0:T(8,128)S(1)} fusion(f32[256,2,4,128]{3,2,1,0:T(4,128)S(1)} %bitcast_multiply_fusion, f32[256,2,4,128]{3,2,1,0:T(4,128)S(1)} %fusion.16, f32[256,8,8]{2,1,0:T(8,128)S(1)} %copy-done.22, f32[256,2,8]{2,1,0:T(2,128)} %copy.621, f32[256,2,8]{2,1,0:T(2,128)S(1)} %copy.615), kind=kOutput, calls=%fused_computation.26 | convolution fusion | flops 51019776 | bytes 2326528 | tf_op jit(solution)/shard_map/bhid,bhjd->bhij/dot_general | solution.py:14
  128.1 3.4 fusion.10
  133.5 15.6 %fusion.22 = f32[256,2,4,32]{3,2,1,0:T(4,128)S(1)} fusion(f32[256,2,32,128]{3,2,1,0:T(8,128)} %param.33, f32[256,4,2,128]{3,2,1,0:T(2,128)S(1)} %reshape.152, f32[256,2,4]{2,1,0:T(2,128)S(1)} %copy.609, f32[256,2,4]{2,1,0:T(2,128)S(1)} %copy.597), kind=kOutput, calls=%fused_computation.58 | convolution fusion | flops 101187584 | bytes 9715712 | tf_op jit(solution)/shard_map/bhid,bhed->bhie/dot_general | solution.py:14
  157.2 10.5 %pad_maximum_fusion.7 = (f32[256,2,1,160]{3,2,1,0:T(1,128)}, f32[256,2,1,160]{3,2,1,0:T(1,128)S(1)}, f32[256,2,1,160]{3,2,1,0:T(1,128)S(1)}, f32[256,2,1,160]{3,...) fusion(f32[256,2,8,128]{3,2,1,0:T(8,128)S(1)} %fusion.8, ...), kind=kLoop, calls=%fused_computation.72 | loop fusion | flops 655360 | bytes 5242880 | tf_op jit(solution)/shard_map/concatenate | solution.py:109
  170.8 7.6 %fusion.24 = f32[256,2,1,160]{3,2,1,0:T(1,128)} fusion(f32[256,2,1,160]{3,2,1,0:T(1,128)S(1)} %copy.650, f32[256,2,1,160]{3,2,1,0:T(1,128)S(1)} %get-tuple-element.41, f32[256,2,8,8]{3,2,1,0:T(8,128)} %copy-done.6), kind=kOutput, calls=%fused_computation.60 | convolution fusion | flops 2129920 | bytes 1245184 | tf_op jit(solution)/shard_map/bhj,bhjd->bhd/dot_general | solution.py:14
  188.9 8.4 %fusion.5 = f32[256,2,1,160]{3,2,1,0:T(1,128)} fusion(f32[256,2,1,160]{3,2,1,0:T(1,128)} %copy.652, f32[256,2,1,160]{3,2,1,0:T(1,128)} %copy.651, f32[256,2,1,160]{3,2,1,0:T(1,128)} %copy-done.8, f32[256,2,1,160]{3,2,1,0:T(1,128)S(1)} %get-tuple-element.41, f32[256,2,8,8]{3,2,1,0:T(8,128)S(1)} %copy-done.7), kind=kOutput, calls=%fused_computation.28 | convolution fusion | flops 4915200 | bytes 2097152 | tf_op jit(solution)/shard_map/bhj,bhjd->bhd/dot_general | solution.py:14
  220.7 11.4 %stack.101 = f32[256,2,7,160]{3,2,1,0:T(8,128)} concatenate(f32[256,2,1,160]{3,2,1,0:T(1,128)S(1)} %get-tuple-element.41, f32[256,2,1,160]{3,2,1,0:T(1,128)S(1)} %copy-done.9, f32[256,2,1,160]{3,2,1,0:T(1,128)} %copy.651, f32[256,2,1,160]{3,2,1,0:T(1,128)} %copy.652, f32[256,2,1,160]{3,2,1,0:T(1,128)} %copy.653, f32[256,2,1,160]{3,2,1,0:T(1,128)} %copy.654, f32[256,2,1,160]{3,2,1,0:T(1,128)} %copy.655), dimensions={2} | concatenate | bytes 4587520 | tf_op jit(solution)/shard_map/stack | solution.py:118
  232.2 7.2 %fusion.48 = f32[256,2,1,160]{3,2,1,0:T(1,128)} fusion(f32[256,2,7,160]{3,2,1,0:T(8,128)} %stack.101, f32[256,2,8,8]{3,2,1,0:T(8,128)S(1)} %copy-done.7), kind=kOutput, calls=%fused_computation.96 | convolution fusion | flops 6881280 | bytes 2883584 | tf_op jit(solution)/shard_map/bhj,bhjd->bhd/dot_general | solution.py:14
  246.2 11.2 %stack.103 = f32[256,2,8,160]{3,2,1,0:T(8,128)} concatenate(f32[256,2,1,160]{3,2,1,0:T(1,128)S(1)} %get-tuple-element.41, f32[256,2,1,160]{3,2,1,0:T(1,128)S(1)} %copy-done.9, f32[256,2,1,160]{3,2,1,0:T(1,128)S(1)} %copy-done.10, f32[256,2,1,160]{3,2,1,0:T(1,128)S(1)} %copy-done.11, f32[256,2,1,160]{3,2,1,0:T(1,128)S(1)} %copy-done.12, f32[256,2,1,160]{3,2,1,0:T(1,128)S(1)} %copy-done.13, ...), dimensions={2} | concatenate | bytes 5242880 | tf_op jit(solution)/shard_map/stack | solution.py:121
  257.4 16.8 %slice_subtract_fusion = f32[256,2,8,32]{3,2,1,0:T(8,128)S(1)} fusion(f32[256,2,8,160]{3,2,1,0:T(8,128)} %stack.103, f32[256,2,32,128]{3,2,1,0:T(8,128)} %param.33), kind=kOutput, calls=%fused_computation.23 | convolution fusion | flops 201457664 | bytes 11534336 | tf_op jit(solution)/shard_map/bhcd,bhed->bhce/dot_general | solution.py:14
  274.3 4.2 convolution_multiply_fusion
  278.6 3.4 fusion.95
  284.3 6.4 %psum.14 = f32[256,2,4]{0,2,1:T(4,128)S(1)} all-reduce(f32[256,2,4]{0,2,1:T(4,128)S(1)} %copy.659), channel_id=1, replica_groups=mesh['kv'=8,'tp'=4] {'tp'}, use_global_device_ids=true, to_apply=%region_5.6 | all-reduce | flops 2048 | bytes 16384 | tf_op jit(solution)/shard_map/psum | solution.py:149
  292.8 4.5 fusion.96
  298.4 18.9 %multiply_add_fusion = f32[256,2,32,128]{3,2,1,0:T(8,128)} fusion(f32[256,2,32,128]{3,2,1,0:T(8,128)} %param.33, f32[256,2]{1,0:T(8,128)S(1)} %bitcast.222, f32[256,2,8,32]{3,2,1,0:T(8,128)S(1)} %slice_subtract_fusion, f32[256,2,4]{2,1,0:T(2,128)S(1)} %copy.666, bf16[256,4,256]{2,1,0:T(4,128)(2,1)S(1)} %copy-done.26, f32[256,2,4]{2,1,0:T(2,128)S(1)} %copy-done.32), kind=kOutput, calls=%fused_computation.19 | convolution fusion | flops 105644032 | bytes 19005440 | tf_op jit(solution)/shard_map/bhcd,bhce->bhed/dot_general | solution.py:14
  317.2 158.6 %all-reduce.4.cloned.1.call-done = f32[1024,2048]{1,0:T(8,128)} async-done(((f32[1024,2048]{1,0:T(8,128)}), f32[1024,2048]{1,0:T(8,128)}) %all-reduce.4.cloned.1.call-update) | async-done | bytes 8388624 | tf_op jit(solution)/shard_map/psum | solution.py:218
  475.8 4.1 multiply_reduce_fusion
  (226 shorter events, 91.0 us)
Async XLA Ops:
  7.2 98.1 %copy-start = (bf16[2048,256]{1,0:T(8,128)(2,1)S(1)}, bf16[2048,256]{1,0:T(8,128)(2,1)}, u32[]{:S(2)}) copy-start(bf16[2048,256]{1,0:T(8,128)(2,1)} %param.23) | copy-start | bytes 3145732
  7.2 7.7 %copy-start.41 = (bf16[256,4,2,32]{0,3,2,1:T(8,128)(2,1)S(1)}, bf16[256,4,2,32]{0,3,2,1:T(8,128)(2,1)}, u32[]{:S(2)}) copy-start(bf16[256,4,2,32]{0,3,2,1:T(8,128)(2,1)} %param.35) | copy-start | bytes 393220
  7.2 8.8 %copy-start.47 = (s32[256]{0:T(256)S(1)}, s32[256]{0:T(256)}, u32[]{:S(2)}) copy-start(s32[256]{0:T(256)} %param.38) | copy-start | bytes 3076
  7.2 8.8 %copy-start.44 = (f32[256,4,2]{0,2,1:T(2,128)S(1)}, f32[256,4,2]{0,2,1:T(2,128)}, u32[]{:S(2)}) copy-start(f32[256,4,2]{0,2,1:T(2,128)} %param.36) | copy-start | bytes 24580
  7.2 8.8 %copy-start.45 = (f32[256,4,2]{0,2,1:T(2,128)S(1)}, f32[256,4,2]{0,2,1:T(2,128)}, u32[]{:S(2)}) copy-start(f32[256,4,2]{0,2,1:T(2,128)} %param.37) | copy-start | bytes 24580
  7.2 68.8 %all-gather.2.cloned.1.call-start = ((), (), s32[]{:S(2)}) async-start(), calls=%async_computation | async-start | bytes 4325376 | tf_op jit(solution)/shard_map/all_gather | solution.py:174
  8.0 467.8 %all-reduce.4.cloned.1.call-start = ((), (), s32[]{:S(2)}) async-start(), calls=%async_computation.1 | async-start | bytes 16777216 | tf_op jit(solution)/shard_map/psum | solution.py:218
  11.4 83.1 %copy-start.21 = (f32[256,8,8]{2,1,0:T(8,128)}, f32[256,8,8]{2,1,0:T(8,128)S(1)}, u32[]{:S(2)}) copy-start(f32[256,8,8]{2,1,0:T(8,128)S(1)} %copy.607) | copy-start | bytes 196612
  13.9 65.3 %copy-start.31 = (f32[256,2,4]{2,1,0:T(2,128)}, f32[256,2,4]{2,1,0:T(2,128)S(1)}, u32[]{:S(2)}) copy-start(f32[256,2,4]{2,1,0:T(2,128)S(1)} %copy.611) | copy-start | bytes 24580
  17.7 97.6 %copy-start.14 = (f32[256,2,4,128]{3,2,1,0:T(4,128)}, f32[256,2,4,128]{3,2,1,0:T(4,128)S(1)}, u32[]{:S(2)}) copy-start(f32[256,2,4,128]{3,2,1,0:T(4,128)S(1)} %fusion.16) | copy-start | bytes 3145732
  82.2 7.9 %copy-start.42 = (bf16[2048,2]{0,1:T(2,128)(2,1)S(1)}, bf16[2048,2]{0,1:T(2,128)(2,1)}, u32[]{:S(2)}) copy-start(bf16[2048,2]{0,1:T(2,128)(2,1)} %param.27) | copy-start | bytes 24580
  112.8 7.9 %copy-start.17 = (f32[256,2,4,128]{3,2,1,0:T(4,128)}, f32[256,2,4,128]{3,2,1,0:T(4,128)S(1)}, u32[]{:S(2)}) copy-start(f32[256,2,4,128]{3,2,1,0:T(4,128)S(1)} %bitcast_multiply_fusion) | copy-start | bytes 3145732
  115.3 9.1 %copy-start.3 = (bf16[1024,2048]{1,0:T(8,128)(2,1)S(1)}, bf16[1024,2048]{1,0:T(8,128)(2,1)}, u32[]{:S(2)}) copy-start(bf16[1024,2048]{1,0:T(8,128)(2,1)} %reshape.134) | copy-start | bytes 12582916
  133.5 15.6 %copy-start.39 = (f32[256,2,4]{2,1,0:T(2,128)}, f32[256,2,4]{2,1,0:T(2,128)S(1)}, u32[]{:S(2)}) copy-start(f32[256,2,4]{2,1,0:T(2,128)S(1)} %copy.597) | copy-start | bytes 24580
  157.2 11.8 %copy-start.34 = (f32[256,2,1,1]{3,2,1,0:T(1,128)S(1)}, f32[256,2,1,1]{3,2,1,0:T(1,128)}, u32[]{:S(2)}) copy-start(f32[256,2,1,1]{3,2,1,0:T(1,128)} %slice.141) | copy-start | bytes 6148
  170.8 7.6 %copy-start.8 = (f32[256,2,1,160]{3,2,1,0:T(1,128)}, f32[256,2,1,160]{3,2,1,0:T(1,128)S(1)}, u32[]{:S(2)}) copy-start(f32[256,2,1,160]{3,2,1,0:T(1,128)S(1)} %copy.650) | copy-start | bytes 983044
  170.8 8.9 %copy-start.29 = (f32[256,2,1,160]{3,2,1,0:T(1,128)S(1)}, f32[256,2,1,160]{3,2,1,0:T(1,128)}, u32[]{:S(2)}) copy-start(f32[256,2,1,160]{3,2,1,0:T(1,128)} %get-tuple-element.43) | copy-start | bytes 983044
  257.3 16.9 %copy-start.16 = (f32[256,2,4,128]{3,2,1,0:T(4,128)S(1)}, f32[256,2,4,128]{3,2,1,0:T(4,128)}, u32[]{:S(2)}) copy-start(f32[256,2,4,128]{3,2,1,0:T(4,128)} %copy-done.14) | copy-start | bytes 3145732
  257.4 16.9 %copy-start.18 = (f32[256,2,4,128]{3,2,1,0:T(4,128)S(1)}, f32[256,2,4,128]{3,2,1,0:T(4,128)}, u32[]{:S(2)}) copy-start(f32[256,2,4,128]{3,2,1,0:T(4,128)} %copy-done.17) | copy-start | bytes 3145732
  257.4 16.9 %copy-start.20 = (f32[256,4,2,128]{3,2,1,0:T(2,128)S(1)}, f32[256,4,2,128]{3,2,1,0:T(2,128)}, u32[]{:S(2)}) copy-start(f32[256,4,2,128]{3,2,1,0:T(2,128)} %copy-done.19) | copy-start | bytes 3145732
  257.4 16.9 %copy-start.25 = (f32[256,2,8,8]{3,2,1,0:T(8,128)S(1)}, f32[256,2,8,8]{3,2,1,0:T(8,128)}, u32[]{:S(2)}) copy-start(f32[256,2,8,8]{3,2,1,0:T(8,128)} %broadcast_subtract_fusion) | copy-start | bytes 393220
  257.4 16.9 %copy-start.35 = (f32[256,4,8]{2,1,0:T(4,128)S(1)}, f32[256,4,8]{2,1,0:T(4,128)}, u32[]{:S(2)}) copy-start(f32[256,4,8]{2,1,0:T(4,128)} %copy.617) | copy-start | bytes 98308
  257.4 16.9 %copy-start.40 = (f32[256,2,4]{2,1,0:T(2,128)S(1)}, f32[256,2,4]{2,1,0:T(2,128)}, u32[]{:S(2)}) copy-start(f32[256,2,4]{2,1,0:T(2,128)} %copy-done.39) | copy-start | bytes 24580
  283.2 9.6 %copy-start.38 = (bf16[2,32,2048]{2,1,0:T(8,128)(2,1)S(1)}, bf16[2,32,2048]{2,1,0:T(8,128)(2,1)}, u32[]{:S(2)}) copy-start(bf16[2,32,2048]{2,1,0:T(8,128)(2,1)} %param.31) | copy-start | bytes 786436
  (28 other events, 99.4 us)
Sparse Core Ops, SparseCore 0:
  10.9 65.0 all-gather.1
  297.4 178.3 all-reduce.3
where the time goes:
time: 496 us; the launch traced here: 489 us
  waiting for transfers between devices  218 us (44%)
  matrix products  108 us (22%)
  local copies, waits for them, and re-layouts  89.5 us (18%)
  other arithmetic  52.6 us (11%)
  between operations  15.5 us (3%)
  blocking collectives  6.36 us (1%)
    psum x1, waiting for transfers between devices, on_device(): totals = lax.psum(partial_out, ('kv', 'tp'))  159 us
    dot_general x10, matrix products, exact_product(): return jnp.einsum(form, left, right, precision=lax.Precision.HIGHEST)  90 us
    all_gather x1, waiting for transfers between devices, on_device(): gathered = lax.all_gather(tokens, ('kv', 'tp'), axis=2, tiled=True)  58.3 us
    another operation x8, local copies, waits for them, and re-layouts, delta_recursion(): solution = jnp.stack(solved, axis=2)  22.3 us
    another operation x2, local copies, waits for them, and re-layouts, delta_recursion(): jnp.stack(solved, axis=2)  12.1 us
    unnamed x110, local copies, waits for them, and re-layouts  11 us
    concatenate x1, other arithmetic, delta_recursion(): jnp.concatenate([beta_all[..., None] * values_all, (beta_all * jnp.exp(ga...  10.5 us
  transfers between devices with their start and end apart: 2, of which 2 were waited for; matrix products, arithmetic and copies ran while one was open for 6% of the time, Pallas kernels for 0%

commit v1 on v0

v1 whole, which is shorter than its diff:
```python
import functools

import jax
import jax.numpy as jnp
from jax import lax
from jax.experimental import pallas as pl
from jax.experimental.pallas import tpu as pltpu
from jax.sharding import PartitionSpec as P

epsilon = 1e-06
GROUP = 16
AXES = ("kv", "tp")


def total(terms):
    terms = list(terms)
    while len(terms) > 1:
        terms = [sum(terms[i : i + 2][1:], terms[i]) for i in range(0, len(terms), 2)]
    return terms[0]


def delta_kernel(
    prop, q_ref, k_ref, ok_ref, v_ref, ov_ref, sc_ref, s_ref, o_ref, sq_ref, out_ref, kt_ref, eg_ref
):
    lanes = s_ref.shape[0]
    vdim = s_ref.shape[2]
    hd = s_ref.shape[3]
    groups = lanes // GROUP
    f32, bf16 = jnp.float32, jnp.bfloat16

    for index, ref in enumerate((ok_ref, k_ref, q_ref)):
        for p in range(prop):
            tile = ref[p * lanes : (p + 1) * lanes, :].astype(f32)
            kt_ref[index * prop + p] = tile.T
    positions = 2 * prop
    square = [jnp.sum(kt_ref[i] * kt_ref[i], axis=0, keepdims=True) for i in range(3 * prop)]
    inv = [lax.rsqrt(x + epsilon) for x in square]
    inv = inv[:positions] + [x * hd ** (-0.5) for x in inv[positions:]]

    def scalar(row, p):
        return sc_ref[0, row : row + 1, p * lanes : (p + 1) * lanes]

    beta = [scalar(0, p) for p in range(prop)] + [scalar(2, p) for p in range(prop)]
    g = [scalar(1, p) for p in range(prop)] + [scalar(3, p) for p in range(prop)]
    parents = [scalar(4, p) for p in range(prop)]
    ancestor = []
    for i in range(prop):
        direct = [jnp.where(parents[i] == float(j), 1.0, 0.0) for j in range(i)]
        row = []
        for j in range(i):
            row.append(total([direct[j]] + [direct[m] * ancestor[m][j] for m in range(j + 1, i)]))
        ancestor.append(row)

    def vis(i, j):
        if i < prop or j < prop:
            return None
        return ancestor[i - prop][j - prop]

    gam = []
    for i in range(positions):
        acc = g[i]
        for j in range(i):
            seen = vis(i, j)
            acc = acc + (g[j] if seen is None else seen * g[j])
        gam.append(acc)
    eg = [jnp.exp(x) for x in gam]

    def decay(i, j):
        value = jnp.exp(jnp.minimum(gam[i] - gam[j], 0.0))
        seen = vis(i, j)
        return value if seen is None else value * seen

    def gram(i, j):
        return jnp.sum(kt_ref[i] * kt_ref[j], axis=0, keepdims=True) * (inv[i] * inv[j])

    dec = {(i, j): decay(i, j) for i in range(positions) for j in range(i)}
    coupling = {(i, j): beta[i] * gram(i, j) * dec[i, j] for (i, j) in dec}
    reach = {}
    for p in range(prop):
        i = prop + p
        for j in range(i + 1):
            value = gram(positions + p, j)
            reach[p, j] = value if j == i else value * dec[i, j]

    last = eg[prop - 1]
    eg_ref[...] = jnp.broadcast_to(last, (lanes, lanes)).T

    lane = lax.broadcasted_iota(jnp.int32, (vdim, lanes), 1)
    inner, outer = lane % GROUP, lane // GROUP
    products = []
    for c in range(groups):
        rows = s_ref[c * GROUP : (c + 1) * GROUP, 0].reshape(GROUP * vdim, hd).astype(bf16)
        tiles = []
        for ref in (ok_ref, k_ref, q_ref):
            for p in range(prop):
                start = p * lanes + c * GROUP
                tiles.append(ref[start : start + GROUP, :])
        keys = jnp.concatenate(tiles, axis=0)
        product = lax.dot_general(
            rows, keys, (((1,), (1,)), ((), ())), preferred_element_type=f32
        )
        wide = []
        for first in range(0, 3 * prop * GROUP, lanes):
            width = min(lanes, 3 * prop * GROUP - first)
            part = product[:, first : first + width]
            chosen = part[:vdim]
            for s in range(1, GROUP):
                mask = (inner if width == lanes else inner[:, :width]) == s
                chosen = jnp.where(mask, part[s * vdim : (s + 1) * vdim], chosen)
            if width < lanes:
                chosen = jnp.concatenate(
                    [chosen, jnp.zeros((vdim, lanes - width), f32)], axis=1
                )
            wide.append(chosen)
        products.append(wide)

    per_tile = lanes // GROUP

    def swap(source, sources, targets):
        shifted = []
        for d in range(groups):
            acc = None
            for a in range(sources):
                t = (a - d) % groups
                if t >= targets:
                    continue
                acc = source[a] if acc is None else jnp.where(outer == t, source[a], acc)
            shifted.append(acc if acc is None or d == 0 else pltpu.roll(acc, d * GROUP, 1))
        results = []
        for t in range(targets):
            acc = None
            for a in range(sources):
                piece = shifted[(a - t) % groups]
                acc = piece if acc is None else jnp.where(outer == a, piece, acc)
            results.append(acc)
        return results

    raw = []
    for tile in range(len(products[0])):
        count = min(per_tile, 3 * prop - tile * per_tile)
        raw += swap([products[c][tile] for c in range(groups)], groups, count)

    update = []
    for i in range(positions):
        source = ov_ref if i < prop else v_ref
        p = i % prop
        value = source[:, p * lanes : (p + 1) * lanes].astype(f32)
        acc = beta[i] * value - (beta[i] * eg[i] * inv[i]) * raw[i]
        for j in range(i):
            acc = acc - coupling[i, j] * update[j]
        update.append(acc)

    for p in range(prop):
        i = prop + p
        acc = (eg[i] * inv[positions + p]) * raw[positions + p]
        for j in range(i + 1):
            acc = acc + reach[p, j] * update[j]
        o_ref[0, :, p * lanes : (p + 1) * lanes] = acc
        sq_ref[0, :, p * lanes : (p + 1) * lanes] = jnp.sum(acc * acc, axis=0, keepdims=True)

    weighted = [
        update[j] * (jnp.exp(gam[prop - 1] - gam[j]) * inv[j]) for j in range(prop)
    ]
    compact = swap(weighted, prop, groups)
    width = prop * GROUP
    narrow = inner[:, :width]
    for c in range(groups):
        tiles = [
            ok_ref[p * lanes + c * GROUP : p * lanes + (c + 1) * GROUP, :] for p in range(prop)
        ]
        keys = jnp.concatenate(tiles, axis=0)
        piece = compact[c][:, :width]
        left = jnp.concatenate(
            [jnp.where(narrow == s, piece, 0.0) for s in range(GROUP)], axis=0
        ).astype(bf16)
        delta = jnp.dot(left, keys, preferred_element_type=f32)
        for s in range(GROUP):
            seq = c * GROUP + s
            out_ref[seq, 0] = (
                s_ref[seq, 0] * eg_ref[seq : seq + 1, :hd] + delta[s * vdim : (s + 1) * vdim]
            )


def delta_call(prop, lanes, q, k, ok, v, ov, scal, state):
    seqs, heads, vdim, hd = state.shape
    tiles = seqs // lanes
    block = prop * lanes
    natural = pl.BlockSpec((block, hd), lambda t, h: (t, h))
    turned = pl.BlockSpec((vdim, block), lambda t, h: (h, t))
    state_spec = pl.BlockSpec((lanes, 1, vdim, hd), lambda t, h: (t, h, 0, 0))
    return pl.pallas_call(
        functools.partial(delta_kernel, prop),
        grid=(tiles, heads),
        in_specs=[
            natural,
            natural,
            natural,
            turned,
            turned,
            pl.BlockSpec((1, 8, block), lambda t, h: (h, 0, t)),
            state_spec,
        ],
        out_specs=[
            pl.BlockSpec((1, vdim, block), lambda t, h: (h, 0, t)),
            pl.BlockSpec((1, 1, block), lambda t, h: (h, 0, t)),
            state_spec,
        ],
        out_shape=[
            jax.ShapeDtypeStruct((heads, vdim, seqs * prop), jnp.float32),
            jax.ShapeDtypeStruct((heads, 1, seqs * prop), jnp.float32),
            jax.ShapeDtypeStruct(state.shape, jnp.float32),
        ],
        scratch_shapes=[
            pltpu.VMEM((3 * prop, hd, lanes), jnp.float32),
            pltpu.VMEM((lanes, lanes), jnp.float32),
        ],
        compiler_params=pltpu.CompilerParams(vmem_limit_bytes=40 * 1024 * 1024),
        cost_estimate=pl.CostEstimate(
            flops=2 * seqs * heads * vdim * hd * 256,
            bytes_accessed=8 * seqs * heads * vdim * hd,
            transcendentals=0,
        ),
    )(q, k, ok, v, ov, scal, state)


def scattered_sum(blended, weight, own):
    f32, bf16 = jnp.float32, jnp.bfloat16
    channels, rows = blended.shape
    kv, tp = lax.axis_size("kv"), lax.axis_size("tp")
    chips = tp // 2
    core = lax.axis_index("tp") % 2
    halves = weight.reshape(channels, kv * chips, 2, own)

    def half(which):
        part = lax.dynamic_index_in_dim(halves, which, 2, keepdims=False)
        return lax.dot_general(
            part.reshape(channels, kv * chips * own),
            blended,
            (((0,), (0,)), ((), ())),
            preferred_element_type=f32,
        )

    pairs = [(i, i ^ 1) for i in range(tp)]
    received = lax.ppermute(half(1 - core).astype(bf16), "tp", pairs)
    summed = (half(core) + received.astype(f32)).astype(bf16).reshape(kv, chips, own, rows)
    if chips == 2:
        x = lax.axis_index("tp") // 2
        across = [(i, i ^ 2) for i in range(tp)]
        other = lax.dynamic_index_in_dim(summed, 1 - x, 1, keepdims=False)
        mine = lax.dynamic_index_in_dim(summed, x, 1, keepdims=False)
        other = lax.ppermute(other, "tp", across)
        summed = (mine.astype(f32) + other.astype(f32)).astype(bf16)
    else:
        groups = [[2 * x + c for x in range(chips)] for c in range(2)]
        parts = lax.all_to_all(summed, "tp", 1, 1, axis_index_groups=groups, tiled=True)
        summed = jnp.sum(parts.astype(f32), axis=1).astype(bf16)
    parts = lax.all_to_all(summed, "kv", 0, 0, tiled=True)
    return jnp.sum(parts.astype(f32), axis=0)


def on_device(
    tokens,
    input_norm_gain,
    query_weight,
    key_weight,
    value_weight,
    output_gate_weight,
    strength_weight,
    decay_weight,
    head_decay_rate,
    proposal_log_decay,
    head_norm_gain,
    output_weight,
    output_norm_gain,
    state,
    previous_keys,
    previous_values,
    previous_log_decay,
    previous_strengths,
    accepted,
    parent,
):
    f32, bf16 = jnp.float32, jnp.bfloat16
    seqs, heads, vdim, hd = state.shape
    prop = parent.shape[1]
    rows = seqs * prop
    width = input_norm_gain.shape[0]
    lanes = min(128, seqs)
    tiles = seqs // lanes

    def order(x):
        tail = x.shape[2:]
        x = x.reshape((tiles, lanes, prop) + tail)
        return x.swapaxes(1, 2).reshape((rows,) + tail)

    own = tokens.shape[2]
    gathered = lax.all_gather(order(tokens), AXES, axis=1, tiled=True)
    features = gathered.astype(f32)
    normed = features * lax.rsqrt(jnp.mean(features * features, axis=-1, keepdims=True) + epsilon)
    normed = (normed * input_norm_gain.astype(f32)).astype(bf16)

    queries = jnp.dot(normed, query_weight, preferred_element_type=f32).astype(bf16)
    keys = jnp.dot(normed, key_weight, preferred_element_type=f32).astype(bf16)
    small = jnp.concatenate(
        [
            value_weight.reshape(width, -1),
            output_gate_weight.reshape(width, -1),
            strength_weight,
            decay_weight,
        ],
        axis=1,
    )
    side = lax.dot_general(
        small, normed, (((0,), (1,)), ((), ())), preferred_element_type=f32
    )
    channels = heads * vdim
    values = side[:channels].astype(bf16)
    zgate = side[channels : 2 * channels].astype(bf16).astype(f32)
    strength = side[2 * channels : 2 * channels + heads]
    decay_pre = side[2 * channels + heads :]

    beta_new = jax.nn.sigmoid(strength)
    g_new = -head_decay_rate[:, None] * jax.nn.softplus(decay_pre) + order(proposal_log_decay).T
    position = jnp.arange(prop, dtype=jnp.int32)
    live = (position[None, :] < accepted[:, None]).astype(f32)[:, :, None]
    beta_old = order(previous_strengths * live).T
    g_old = order(previous_log_decay * live).T
    parents = jnp.broadcast_to(order(parent).astype(f32)[None], (heads, rows))
    zero = jnp.zeros((heads, rows), f32)
    scal = jnp.stack([beta_old, g_old, beta_new, g_new, parents, zero, zero, zero], axis=1)
    old_keys = order(previous_keys)
    old_values = order(previous_values).reshape(rows, channels).T

    readout, squares, accepted_state = delta_call(
        prop, lanes, queries, keys, old_keys, values, old_values, scal, state
    )
    squares = lax.psum(squares.reshape(heads, rows), "tp")
    scale = lax.rsqrt(squares / hd + epsilon)[:, None, :]
    blended = readout * scale * head_norm_gain.astype(f32)[None, :, None]
    blended = blended * jax.nn.silu(zgate).reshape(heads, vdim, rows)
    blended = blended.reshape(channels, rows).astype(bf16)
    share = scattered_sum(blended, output_weight.reshape(channels, width), own)
    sumsq = lax.psum(jnp.sum(share * share, axis=0), AXES)
    scaling = lax.rsqrt(sumsq / width + epsilon)[None, :]
    layer_out = (share * scaling * output_norm_gain.astype(f32)[:, None]).astype(bf16).T
    layer_out = layer_out.reshape(tiles, prop, lanes, own).swapaxes(1, 2)
    return (layer_out.reshape(seqs, prop, own), accepted_state)


def solution(mesh):
    placed = (
        P(None, None, AXES),
        P(),
        P(None, "kv"),
        P(None, "kv"),
        P(None, "kv", "tp"),
        P(None, "kv", "tp"),
        P(None, "kv"),
        P(None, "kv"),
        P("kv"),
        P(None, None, "kv"),
        P("tp"),
        P("kv", "tp", None),
        P(AXES),
        P(None, "kv", "tp", None),
        P(None, None, "kv"),
        P(None, None, "kv", "tp"),
        P(None, None, "kv"),
        P(None, None, "kv"),
        P(),
        P(),
    )
    return jax.shard_map(
        on_device,
        mesh=mesh,
        in_specs=placed,
        out_specs=(P(None, None, AXES), P(None, "kv", "tp", None)),
        check_vma=False,
    )
```

time: 496 us -> 218 us (0.44); the launches traced: 489 us -> 216 us
  waiting for transfers between devices: 218 us -> 108 us
  matrix products: 108 us -> 11.3 us
  local copies, waits for them, and re-layouts: 89.5 us -> 13.8 us
  other arithmetic: 52.6 us -> 10.6 us
  blocking collectives: 6.36 us -> 44.4 us
  Pallas kernels: 0 us -> 9.3 us
    psum x1 -> x0, waiting for transfers between devices: 159 us -> none  [on_device(): totals = lax.psum(partial_out, ('kv', 'tp'))]
    dot_general x17 -> x5, matrix products: 108 us -> 11.3 us  [the longest x1 4.09 us: on_device(): keys = jnp.dot(normed, key_weight, preferred_element_type=f32).astype(bf16)]
    psum x1 -> x2, blocking collectives: 6.36 us -> 44.4 us  [the longest x1 37.5 us: on_device(): sumsq = lax.psum(jnp.sum(share * share, axis=0), AXES)]
    another operation x10, local copies, waits for them, and re-layouts: 34.4 us -> 1.76 us  [the longest x1 1.53 us: scattered_sum(): halves = weight.reshape(channels, kv * chips, 2, own)]
    ppermute x0 -> x2, waiting for transfers between devices: none -> 28.1 us  [the longest x1 24.7 us: scattered_sum(): other = lax.ppermute(other, 'tp', across)]
    all_to_all x0 -> x1, waiting for transfers between devices: none -> 25.5 us  [scattered_sum(): parts = lax.all_to_all(summed, 'kv', 0, 0, tiled=True)]
    slice x15 -> x1, local copies, waits for them, and re-layouts: 11.7 us -> 0.01 us  [on_device(): values = side[:channels].astype(bf16)]
    concatenate x3 -> x0, other arithmetic: 10.5 us -> none  [the longest x1 10.5 us: delta_recursion(): jnp.concatenate([beta_all[..., None] * values_all, (beta_all * jnp.exp(ga...]
  transfers between devices with their start and end apart: 2 -> 4, of which waited for: 2 -> 4; matrix products, arithmetic and copies ran while one was open for 6% -> 6% of each run, Pallas kernels for 0% -> 0%
where the time goes in v1:
time: 218 us; the launch traced here: 216 us
  waiting for transfers between devices  108 us (50%)
  blocking collectives  44.4 us (20%)
  between operations  14.5 us (7%)
  local copies, waits for them, and re-layouts  13.8 us (6%)
  matrix products  11.3 us (5%)
  other arithmetic  10.6 us (5%)
  Pallas kernels  9.3 us (4%)
  starting transfers between devices  4.49 us (2%)
    all_gather x1, waiting for transfers between devices, on_device(): gathered = lax.all_gather(order(tokens), AXES, axis=1, tiled=True)  54.5 us
    psum x1, blocking collectives, on_device(): sumsq = lax.psum(jnp.sum(share * share, axis=0), AXES)  37.5 us
    all_to_all x1, waiting for transfers between devices, scattered_sum(): parts = lax.all_to_all(summed, 'kv', 0, 0, tiled=True)  25.5 us
    ppermute x1, waiting for transfers between devices, scattered_sum(): other = lax.ppermute(other, 'tp', across)  24.7 us
    pallas_call x1, Pallas kernels, delta_call(): pl.pallas_call(functools.partial(delta_kernel, prop), grid=(tiles, heads)...  9.3 us
    psum x1, blocking collectives, on_device(): squares = lax.psum(squares.reshape(heads, rows), 'tp')  6.85 us
  transfers between devices with their start and end apart: 4, of which 4 were waited for; matrix products, arithmetic and copies ran while one was open for 6% of the time, Pallas kernels for 0%

profile of v1, /device:TPU:0, one launch (start us, length us, event | category | flops | bytes accessed | tf_op | source)
XLA Modules:
  0.0 216.4 jit_solution(10820136725009665674)
XLA Ops:
  7.2 1.1 reshape.113
  14.2 0.9 reshape.119
  15.5 1.5 reshape_reshape.6
  17.0 3.5 %dynamic-slice_reduce_fusion = (bf16[64,16,64]{2,1,0:T(8,128)(2,1)S(1)}, bf16[64,16,64]{2,1,0:T(8,128)(2,1)S(1)}) fusion(bf16[64,16,2,64]{3,2,1,0:T(2,128)(2,1)S(1)} %reshape_reshape.6, s32[]{:T(128)S(6)} %select_n.32, s32[]{:T(128)S(6)} %select_n.30), kind=kLoop, calls=%fused_computation.21 | loop fusion | bytes 524296 | tf_op jit(solution)/shard_map/jit(dynamic_index_in_dim)/dynamic_slice | solution.py:235
  20.5 0.9 reshape.128
  21.4 54.5 %all-gather.2.cloned.1.call-done = bf16[1024,2048]{0,1:T(8,128)(2,1)} async-done(((bf16[1024,64]{0,1:T(8,128)(2,1)}), bf16[1024,2048]{0,1:T(8,128)(2,1)}) %all-gather.2.cloned.1.call-update) | async-done | bytes 4194320 | tf_op jit(solution)/shard_map/all_gather | solution.py:297
  75.9 3.3 %fusion = f32[1024]{0:T(1024)S(1)} fusion(bf16[1024,2048]{0,1:T(8,128)(2,1)} %all-gather.2.cloned.1.call-done), kind=kLoop, calls=%fused_computation.2 | loop fusion | flops 6290432 | bytes 4198400 | tf_op jit(solution)/shard_map/reduce_sum | solution.py:299
  79.4 1.4 fusion.26
  81.2 4.1 %convolution_convert_fusion.1.k_ref = bf16[1024,256]{1,0:T(8,128)(2,1)S(1)} fusion(bf16[2048,256]{1,0:T(8,128)(2,1)S(1)} %copy-done, bf16[1024,2048]{0,1:T(8,128)(2,1)} %all-gather.2.cloned.1.call-done, f32[2048]{0:T(1024)S(1)} %convert_element_type.84, f32[1024]{0:T(1024)S(1)} %add_rsqrt_fusion.2), kind=kOutput, calls=%fused_computation.10 | convolution fusion | flops 1082392576 | bytes 5779456 | tf_op jit(solution)/shard_map/dot_general | solution.py:303
  85.3 1.8 convolution_convert_fusion.2.q_ref
  87.7 9.3 %shard_map.203 = (f32[2,32,1024]{2,1,0:T(8,128)S(1)}, f32[2,1,1024]{2,1,0:T(1,128)S(1)}, f32[256,2,32,128]{3,2,1,0:T(8,128)}) custom-call(bf16[1024,256]{1,0:T(8,128)(2,1)S(1)} %convolution_convert_fusion.2.q_ref, bf16[1024,256]{1,0:T(8,128)(2,1)S(1)} %convolution_convert_fusion.1.k_ref, bf16[1024,256]{1,0:T(8,128)(2,1)S(1)} %bitcast.79, ...), custom_call_target="tpu_custom_call" | custom-call | flops 1073741824 | bytes 16777216 | tf_op jit(solution)/shard_map/pallas_call | solution.py:191
  97.0 6.9 %psum.14 = f32[2,1024]{1,0:T(2,128)S(1)} all-reduce(f32[2,1024]{1,0:T(2,128)S(1)} %bitcast.95), channel_id=1, replica_groups=mesh['kv'=8,'tp'=4] {'tp'}, use_global_device_ids=true, to_apply=%region_1.2 | all-reduce | flops 2048 | bytes 16384 | tf_op jit(solution)/shard_map/psum | solution.py:337
  104.0 1.6 convolution_convert_fusion
  105.7 0.9 reshape.112
  106.6 3.4 %collective-permute-done = bf16[1024,1024]{1,0:T(8,128)(2,1)} collective-permute-done((bf16[1024,1024]{1,0:T(8,128)(2,1)S(1)}, bf16[1024,1024]{1,0:T(8,128)(2,1)}, u32[]{:S(2)}, u32[]{:S(2)}) %collective-permute-start) | collective-permute-done | bytes 2097184 | tf_op jit(solution)/shard_map/ppermute | solution.py:244
  110.0 2.4 %add_convert_fusion = bf16[1024,1024]{1,0:T(8,128)(2,1)S(1)} fusion(bf16[1024,1024]{1,0:T(8,128)(2,1)} %collective-permute-done, bf16[64,1024]{1,0:T(8,128)(2,1)} %reshape.112, bf16[64,1024]{1,0:T(8,128)(2,1)S(1)} %bitcast.84), kind=kOutput, calls=%fused_computation.5 | convolution fusion | flops 137363456 | bytes 4456448 | tf_op jit(solution)/shard_map/dot_general | solution.py:236
  112.4 1.1 dynamic-slice_bitcast_fusion
  113.5 0.8 collective-permute-start.1
  114.3 24.7 %collective-permute-done.1 = bf16[8,64,1024]{2,1,0:T(8,128)(2,1)} collective-permute-done((bf16[8,64,1024]{2,1,0:T(8,128)(2,1)}, bf16[8,64,1024]{2,1,0:T(8,128)(2,1)}, u32[]{:S(2)}, u32[]{:S(2)}) %collective-permute-start.1) | collective-permute-done | bytes 1048608 | tf_op jit(solution)/shard_map/ppermute | solution.py:251
  139.1 2.6 %fusion.3 = bf16[8,64,1024]{2,1,0:T(8,128)(2,1)} fusion(bf16[8,64,1024]{2,1,0:T(8,128)(2,1)} %collective-permute-done.1, bf16[8,2,64,1024]{3,2,1,0:T(8,128)(2,1)S(1)} %bitcast.82, s32[]{:T(128)S(6)} %select_n.34), kind=kLoop, calls=%fused_computation.7 | loop fusion | flops 2097152 | bytes 3145732 | tf_op jit(solution)/shard_map/convert_element_type | solution.py:252
  141.7 3.6 %all-to-all-start = ((bf16[8,64,1024]{2,1,0:T(8,128)(2,1)}), bf16[8,64,1024]{2,1,0:T(8,128)(2,1)S(1)}, u32[]{:S(2)}, u32[]{:S(2)}) async-start(bf16[8,64,1024]{2,1,0:T(8,128)(2,1)} %fusion.3), calls=%async_computation | async-start | bytes 2097152 | tf_op jit(solution)/shard_map/all_to_all | solution.py:257
  145.3 25.5 %all-to-all-done = bf16[8,64,1024]{2,1,0:T(8,128)(2,1)S(1)} async-done(((bf16[8,64,1024]{2,1,0:T(8,128)(2,1)}), bf16[8,64,1024]{2,1,0:T(8,128)(2,1)S(1)}, u32[]{:S(2)}, u32[]{:S(2)}) %all-to-all-start) | async-done | bytes 1048608 | tf_op jit(solution)/shard_map/all_to_all | solution.py:257
  171.0 37.5 %psum.15 = f32[1024]{0:T(1024)S(1)} all-reduce(f32[1024]{0:T(1024)S(1)} %multiply_reduce_fusion), channel_id=1, replica_groups=mesh['kv'=8,'tp'=4] {'kv','tp'}, use_global_device_ids=true, to_apply=%region_4.5 | all-reduce | flops 1024 | bytes 8192 | tf_op jit(solution)/shard_map/psum | solution.py:343
  208.8 0.7 reshape.131
  (70 shorter events, 8.0 us)
Async XLA Ops:
  7.2 74.0 %copy-start = (bf16[2048,256]{1,0:T(8,128)(2,1)S(1)}, bf16[2048,256]{1,0:T(8,128)(2,1)}, u32[]{:S(2)}) copy-start(bf16[2048,256]{1,0:T(8,128)(2,1)} %param.23) | copy-start | bytes 3145732
  7.2 14.2 %copy-start.3 = (bf16[256,4,256]{2,1,0:T(4,128)(2,1)S(1)}, bf16[256,4,256]{2,1,0:T(4,128)(2,1)}, u32[]{:S(2)}) copy-start(bf16[256,4,256]{2,1,0:T(4,128)(2,1)} %param.34) | copy-start | bytes 1572868
  7.2 68.7 %all-gather.2.cloned.1.call-start = ((), (), s32[]{:S(2)}) async-start(), calls=%async_computation.1 | async-start | bytes 4325376 | tf_op jit(solution)/shard_map/all_gather | solution.py:297
  15.3 63.9 %copy-start.5 = (bf16[2048,2,32]{0,2,1:T(8,128)(2,1)S(1)}, bf16[2048,2,32]{0,2,1:T(8,128)(2,1)}, u32[]{:S(2)}) copy-start(bf16[2048,2,32]{0,2,1:T(8,128)(2,1)} %param.25) | copy-start | bytes 786436
  15.4 63.9 %copy-start.6 = (bf16[2048,2,32]{0,2,1:T(8,128)(2,1)S(1)}, bf16[2048,2,32]{0,2,1:T(8,128)(2,1)}, u32[]{:S(2)}) copy-start(bf16[2048,2,32]{0,2,1:T(8,128)(2,1)} %param.24) | copy-start | bytes 786436
  15.4 63.9 %copy-start.7 = (bf16[2048,2]{0,1:T(2,128)(2,1)S(1)}, bf16[2048,2]{0,1:T(2,128)(2,1)}, u32[]{:S(2)}) copy-start(bf16[2048,2]{0,1:T(2,128)(2,1)} %param.27) | copy-start | bytes 24580
  15.4 63.9 %copy-start.8 = (bf16[2048,2]{0,1:T(2,128)(2,1)S(1)}, bf16[2048,2]{0,1:T(2,128)(2,1)}, u32[]{:S(2)}) copy-start(bf16[2048,2]{0,1:T(2,128)(2,1)} %param.26) | copy-start | bytes 24580
  75.9 3.4 %copy-start.1 = (bf16[1024,2048]{0,1:T(8,128)(2,1)S(1)}, bf16[1024,2048]{0,1:T(8,128)(2,1)}, u32[]{:S(2)}) copy-start(bf16[1024,2048]{0,1:T(8,128)(2,1)} %all-gather.2.cloned.1.call-done) | copy-start | bytes 12582916
  81.1 4.1 %copy-start.2 = (bf16[1024,2048]{0,1:T(8,128)(2,1)S(1)}, bf16[1024,2048]{0,1:T(8,128)(2,1)}, u32[]{:S(2)}) copy-start(bf16[1024,2048]{0,1:T(8,128)(2,1)} %all-gather.2.cloned.1.call-done) | copy-start | bytes 12582916
  81.1 4.1 %copy-start.4 = (bf16[2048,256]{1,0:T(8,128)(2,1)S(1)}, bf16[2048,256]{1,0:T(8,128)(2,1)}, u32[]{:S(2)}) copy-start(bf16[2048,256]{1,0:T(8,128)(2,1)} %param.22) | copy-start | bytes 3145732
  81.2 5.9 %slice-start = ((s8[8388608]{0:T(1024)(128)(4,1)}), s8[4194304]{0:T(1024)(128)(4,1)S(1)}, s32[]{:S(2)}) async-start(s8[8388608]{0:T(1024)(128)(4,1)} %bitcast.77), calls=%async_computation.2 | async-start | bytes 8388608
  85.3 2.4 %slice-start.1 = ((s8[8388608]{0:T(1024)(128)(4,1)}), s8[4194304]{0:T(1024)(128)(4,1)S(1)}, s32[]{:S(2)}) async-start(s8[8388608]{0:T(1024)(128)(4,1)} %bitcast.77), calls=%async_computation.3 | async-start | bytes 8388608
  105.6 4.4 %collective-permute-start = (bf16[1024,1024]{1,0:T(8,128)(2,1)S(1)}, bf16[1024,1024]{1,0:T(8,128)(2,1)}, u32[]{:S(2)}, u32[]{:S(2)}) collective-permute-start(bf16[1024,1024]{1,0:T(8,128)(2,1)S(1)} %convolution_convert_fusion), channel_id=1, source_target_pairs={{0,1},{1,0},{2,3},{3,2},{4,5},{5,4},{6,7},{7,6},{8,9},{9,8},{10,11... | collective-permute-start | bytes 6291464 | tf_op jit(solution)/shard_map/ppermute | solution.py:244
  112.4 32.9 %copy-start.9 = (bf16[64]{0:T(256)(128)(2,1)S(1)}, bf16[64]{0:T(256)(128)(2,1)}, u32[]{:S(2)}) copy-start(bf16[64]{0:T(256)(128)(2,1)} %param.32) | copy-start | bytes 388
  113.5 25.5 %collective-permute-start.1 = (bf16[8,64,1024]{2,1,0:T(8,128)(2,1)}, bf16[8,64,1024]{2,1,0:T(8,128)(2,1)}, u32[]{:S(2)}, u32[]{:S(2)}) collective-permute-start(bf16[8,64,1024]{2,1,0:T(8,128)(2,1)} %dynamic-slice_bitcast_fusion), channel_id=1, source_target_pairs={{0,2},{1,3},{2,0},{3,1},{4,6},{5,7},{6,4},{7,5},{8,10},{9,11},{10,... | collective-permute-start | bytes 3145736 | tf_op jit(solution)/shard_map/ppermute | solution.py:251
  141.7 29.1 %all-to-all-start = ((bf16[8,64,1024]{2,1,0:T(8,128)(2,1)}), bf16[8,64,1024]{2,1,0:T(8,128)(2,1)S(1)}, u32[]{:S(2)}, u32[]{:S(2)}) async-start(bf16[8,64,1024]{2,1,0:T(8,128)(2,1)} %fusion.3), calls=%async_computation | async-start | bytes 2097152 | tf_op jit(solution)/shard_map/all_to_all | solution.py:257
Sparse Core Ops, SparseCore 0:
  11.4 64.4 all-gather.1
